TPU v7x, 32 devices: a whole 2x2x4 slice. The times are simulated.
32 devices in a mesh: ep: 8 (over z, x), tp: 4 (over y, core).
Axes of the slice: x: 2, y: 2, z: 4, core: 2. Of those that a mesh axis runs over, the one named last changes fastest.
Arguments:
- mix_input: bfloat16 [3072, 2048], P('ep', 'tp'), may hold values from -6 to 6
- mix_gain: float32 [2048], replicated, may hold values from 0.1 to 1.9
- gate_b_weight: bfloat16 [2048, 2048], P(None, 'tp'), may hold values from -0.125 to 0.125
- gate_c_weight: bfloat16 [2048, 2048], P(None, 'tp'), may hold values from -0.125 to 0.125
- value_weight: bfloat16 [2048, 2048], P(None, 'tp'), may hold values from -0.125 to 0.125
- conv_weight: float32 [3, 2048], P(None, 'tp'), may hold values from -3 to 3
- out_weight: bfloat16 [2048, 2048], P('tp'), may hold values from -0.125 to 0.125
- expert_input: bfloat16 [1280, 2048], P('ep', 'tp'), may hold values from -6 to 6
- expert_gain: float32 [2048], replicated, may hold values from 0.1 to 1.9
- routes: int32 [1280, 2], P('ep'), may hold values from 0 to 7, all different within a row; in each aligned block of 160 rows (0 to 159, 160 to 319, ...) at most 80 rows name the same one
- route_weight: float32 [1280, 2], P('ep'), may hold values from 0.2 to 1
- expert_gate: bfloat16 [8, 2048, 3072], P('ep', None, 'tp'), may hold values from -0.125 to 0.125
- expert_up: bfloat16 [8, 2048, 3072], P('ep', None, 'tp'), may hold values from -0.125 to 0.125
- expert_down: bfloat16 [8, 3072, 2048], P('ep', 'tp'), may hold values from -0.109375 to 0.109375
Outputs:
- mix_output: bfloat16 [3072, 2048], P('ep', 'tp')
- expert_output: bfloat16 [1280, 2048], P('ep', 'tp')
Inputs may be any that keep to these rules, and one draw needn't show every extreme that they name: `routes`: the 2 experts of a row differ. Among the rows of one device no expert is named more than 80 times, a bound that some block reaches.
All inputs are finite; a program needn't handle non-finite values.
Results may differ from a plain program's by a relative error of at most 0.019.
Values may be sent and summed in bfloat16 or wider, within the bound.
No kernel may reach another device: no remote copies, remote signals or barrier semaphores. Data moves between devices by JAX's collectives and lax.ppermute only.
A program may use at most 64 MiB of HBM per device.

v0:
```python
import jax
import jax.numpy as jnp
from jax import lax
from jax.sharding import PartitionSpec as P

epsilon = 1e-06
routed_scale = 2.5


def passed_along(block, axis, distance):
    devices = range(lax.axis_size(axis))
    route = [(i - distance, i) for i in devices if i - distance in devices]
    return lax.ppermute(block, axis, route)


def project_piece(piece, gain_vector, matrices, group_count):
    widened = piece.astype(jnp.float32)
    columns = piece.shape[-1]
    scaled = (widened * gain_vector).astype(jnp.bfloat16)
    grouped = scaled.reshape(group_count, -1, columns)
    updated = tuple(
        (
            jnp.einsum("gsd,gdf->gsf", grouped, matrix, preferred_element_type=jnp.float32)
            for matrix in matrices
        )
    )
    return (updated, jnp.sum(widened * widened, axis=-1))


def local(
    mix_input,
    mix_gain,
    gate_b_weight,
    gate_c_weight,
    value_weight,
    conv_weight,
    out_weight,
    expert_input,
    expert_gain,
    routes,
    route_weight,
    expert_gate,
    expert_up,
    expert_down,
):
    ep_count = lax.axis_size("ep")
    local_experts = expert_gate.shape[0]
    model_width = mix_gain.shape[0]
    expert_count = local_experts * ep_count
    tok_local, top_count = routes.shape
    capacity = 2 * tok_local * top_count // expert_count
    feature_local = expert_input.shape[1]
    mix_rows = mix_input.shape[0]
    slot_rows = ep_count * capacity
    flat_routes = routes.reshape(-1)
    pair_count = flat_routes.shape[0]
    matches = (
        flat_routes[:, None] == lax.broadcasted_iota(jnp.int32, (pair_count, expert_count), 1)
    ).astype(jnp.int32)
    ranks = jnp.sum((jnp.cumsum(matches, axis=0) - matches) * matches, axis=1)
    slot_iota = lax.broadcasted_iota(jnp.int32, (pair_count, expert_count * capacity), 1)
    send_table = (slot_iota == (flat_routes * capacity + ranks)[:, None]).astype(jnp.bfloat16)
    back_index = (
        flat_routes % local_experts * slot_rows + flat_routes // local_experts * capacity + ranks
    )
    back_table = (slot_iota == back_index[:, None]).astype(jnp.bfloat16)
    repeated = jnp.repeat(expert_input, top_count, axis=0)
    outgoing = lax.dot_general(
        send_table, repeated, (((0,), (0,)), ((), ())), preferred_element_type=jnp.float32
    ).astype(jnp.bfloat16)
    outgoing = outgoing.reshape(ep_count, local_experts, capacity, feature_local)
    arrived = lax.all_to_all(outgoing, "ep", split_axis=0, concat_axis=2, tiled=True)
    arrived = arrived.reshape(local_experts * slot_rows, feature_local)
    mix_weights = (gate_b_weight[None], gate_c_weight[None], value_weight[None])
    expert_weights = (expert_gate, expert_up)
    mix_carry = project_piece(
        lax.all_gather(mix_input, "tp", axis=1, tiled=True), mix_gain, mix_weights, 1
    )
    expert_carry = project_piece(
        lax.all_gather(arrived, "tp", axis=1, tiled=True),
        expert_gain,
        expert_weights,
        local_experts,
    )
    mix_totals, mix_squares = mix_carry
    mix_factor = lax.rsqrt(mix_squares / model_width + epsilon)[:, None]
    outer_gate = mix_totals[0][0] * mix_factor
    product = mix_totals[1][0] * mix_factor * (mix_totals[2][0] * mix_factor)
    edge_rows = passed_along(product[mix_rows - 2 :], "ep", 1)
    padded = jnp.concatenate([edge_rows, product], axis=0)
    convolved = (
        conv_weight[0] * padded[:mix_rows]
        + conv_weight[1] * padded[1 : mix_rows + 1]
        + conv_weight[2] * padded[2:]
    )
    gated = (outer_gate * convolved).astype(jnp.bfloat16)
    expert_totals, expert_squares = expert_carry
    expert_factor = lax.rsqrt(expert_squares / model_width + epsilon).reshape(
        local_experts, slot_rows, 1
    )
    activated = (
        jax.nn.silu(expert_totals[0] * expert_factor) * (expert_totals[1] * expert_factor)
    ).astype(jnp.bfloat16)
    sliced = out_weight
    mix_sum = lax.psum_scatter(
        lax.dot_general(
            sliced, gated, (((0,), (1,)), ((), ())), preferred_element_type=jnp.float32
        ).astype(jnp.bfloat16),
        "tp",
        scatter_dimension=0,
        tiled=True,
    ).astype(jnp.float32)
    sliced = expert_down
    summed = jnp.einsum("gsf,gfd->dgs", activated, sliced, preferred_element_type=jnp.float32)
    expert_sum = lax.psum_scatter(
        summed.reshape(lax.axis_size("tp") * feature_local, local_experts * slot_rows).astype(
            jnp.bfloat16
        ),
        "tp",
        scatter_dimension=0,
        tiled=True,
    )
    mix_output = mix_sum.T.astype(jnp.bfloat16)
    returning = expert_sum.reshape(feature_local, local_experts, ep_count, capacity)
    returned = lax.all_to_all(returning, "ep", split_axis=2, concat_axis=2, tiled=True)
    returned = returned.reshape(feature_local, local_experts * slot_rows)
    picked = lax.dot_general(
        returned, back_table, (((1,), (1,)), ((), ())), preferred_element_type=jnp.float32
    ).reshape(feature_local, tok_local, top_count)
    normalized = route_weight / jnp.sum(route_weight, axis=1, keepdims=True) * routed_scale
    expert_output = jnp.sum(picked * normalized[None], axis=2).T.astype(jnp.bfloat16)
    return (mix_output, expert_output)


def solution(mesh):
    in_specs = (
        P("ep", "tp"),
        P(),
        P(None, "tp"),
        P(None, "tp"),
        P(None, "tp"),
        P(None, "tp"),
        P("tp", None),
        P("ep", "tp"),
        P(),
        P("ep", None),
        P("ep", None),
        P("ep", None, "tp"),
        P("ep", None, "tp"),
        P("ep", "tp", None),
    )
    out_specs = (P("ep", "tp"), P("ep", "tp"))
    return jax.shard_map(local, mesh=mesh, in_specs=in_specs, out_specs=out_specs, check_vma=False)
```

profile of v0, /device:TPU:0, one launch (start us, length us, event | category | flops | bytes accessed | tf_op | source)
XLA Modules:
  0.0 158.1 jit_solution(9475336010663980682)
XLA Ops:
  7.2 0.9 copy.20
  8.3 0.9 reduce-window.6
  9.6 1.1 broadcast_in_dim.2
  10.7 0.8 reshape.158
  11.5 1.6 %convolution_convert_fusion.2 = bf16[640,512]{1,0:T(8,128)(2,1)S(1)} fusion(bf16[320,512]{1,0:T(8,128)(2,1)} %reshape.158, s32[320]{0:T(512)S(1)} %multiply_add_fusion), kind=kOutput, calls=%fused_computation.18 | convolution fusion | flops 210247680 | bytes 984320 | tf_op jit(solution)/shard_map/dot_general | solution.py:68
  13.1 24.9 %all_to_all.14 = bf16[8,1,80,512]{3,2,1,0:T(8,128)(2,1)} all-to-all(bf16[8,1,80,512]{3,2,1,0:T(8,128)(2,1)S(1)} %bitcast.51), channel_id=1, replica_groups=mesh['ep'=8,'tp'=4] {'ep'}, dimensions={0} | all-to-all | bytes 1310720 | tf_op jit(solution)/shard_map/all_to_all | solution.py:72
  38.1 0.7 all-gather.3.cloned.1.call-update
  38.8 23.6 %all-gather.5.cloned.1.call-done = bf16[640,2048]{1,0:T(8,128)(2,1)} async-done(((bf16[640,512]{1,0:T(8,128)(2,1)}), bf16[640,2048]{1,0:T(8,128)(2,1)}) %all-gather.5.cloned.1.call-update) | async-done | bytes 2621456 | tf_op jit(solution)/shard_map/all_gather | solution.py:80
  62.4 2.5 %fusion.1 = f32[640]{0:T(1024)S(1)} fusion(bf16[640,2048]{1,0:T(8,128)(2,1)} %all-gather.5.cloned.1.call-done), kind=kLoop, calls=%fused_computation.3 | loop fusion | flops 3931520 | bytes 2624000 | tf_op jit(solution)/shard_map/reduce_sum | solution.py:27
  64.9 5.4 %fusion.5 = f32[640,768]{1,0:T(8,128)} fusion(bf16[1,2048,768]{2,1,0:T(8,128)(2,1)} %param.26, bf16[640,2048]{1,0:T(8,128)(2,1)S(1)} %copy-done.1, f32[2048]{0:T(1024)S(1)} %copy-done.7), kind=kOutput, calls=%fused_computation.10 | convolution fusion | flops 2017198080 | bytes 7741440 | tf_op jit(solution)/shard_map/gsd,gdf->gsf/dot_general | solution.py:23
  70.4 10.0 %fusion.9 = bf16[2048,640]{0,1:T(8,128)(2,1)} fusion(bf16[1,768,2048]{2,1,0:T(8,128)(2,1)S(1)} %copy-done, f32[640,768]{1,0:T(8,128)} %fusion.5, bf16[1,2048,768]{2,1,0:T(8,128)(2,1)} %param.25, bf16[640,2048]{1,0:T(8,128)(2,1)} %all-gather.5.cloned.1.call-done, f32[2048]{0:T(1024)S(1)} %copy-done.7, f32[640]{0:T(1024)S(1)} %add_rsqrt_fusion), kind=kOutput, calls=%fused_computation.14 | convolution fusion | flops 4035706880 | bytes 13511168 | tf_op jit(solution)/shard_map/gsf,gfd->dgs/dot_general | solution.py:114
  80.4 3.2 %all-gather.3.cloned.1.call-done = bf16[384,2048]{1,0:T(8,128)(2,1)} async-done(((bf16[384,512]{1,0:T(8,128)(2,1)}), bf16[384,2048]{1,0:T(8,128)(2,1)}) %all-gather.3.cloned.1.call-update) | async-done | bytes 1572880 | tf_op jit(solution)/shard_map/all_gather | solution.py:77
  83.6 1.8 %fusion.3 = f32[384]{0:T(512)S(1)} fusion(bf16[384,2048]{1,0:T(8,128)(2,1)} %all-gather.3.cloned.1.call-done), kind=kLoop, calls=%fused_computation.8 | loop fusion | flops 2358912 | bytes 1574400 | tf_op jit(solution)/shard_map/reduce_sum | solution.py:27
  85.5 3.2 %convolution_multiply_fusion = f32[384,512]{1,0:T(8,128)S(1)} fusion(bf16[2048,512]{1,0:T(8,128)(2,1)} %param.18, bf16[384,2048]{1,0:T(8,128)(2,1)} %all-gather.3.cloned.1.call-done, f32[2048]{0:T(1024)S(1)} %copy-done.8, f32[384]{0:T(512)S(1)} %add_rsqrt_fusion.1), kind=kOutput, calls=%fused_computation.19 | convolution fusion | flops 807862272 | bytes 4466176 | tf_op jit(solution)/shard_map/gsd,gdf->gsf/dot_general | solution.py:23
  88.7 1.0 fusion.19
  89.7 3.4 %collective-permute-start = (f32[2,512]{1,0:T(2,128)S(1)}, f32[2,512]{1,0:T(2,128)S(1)}, u32[]{:S(2)}, u32[]{:S(2)}) collective-permute-start(f32[2,512]{1,0:T(2,128)S(1)} %slice.36), channel_id=1, source_target_pairs={{0,4},{4,8},{8,12},{12,16},{16,20},{20,24},{24,28},{1,5},{5,9},{9,... | collective-permute-start | bytes 12296 | tf_op jit(solution)/shard_map/ppermute | solution.py:13
  93.1 1.3 collective-permute-done
  94.4 6.7 %fusion.12 = bf16[2048,384]{0,1:T(8,128)(2,1)} fusion(bf16[512,2048]{1,0:T(8,128)(2,1)} %param.20, f32[2,512]{1,0:T(2,128)S(1)} %collective-permute-done, f32[384,512]{1,0:T(8,128)} %copy-done.5, bf16[2048,512]{1,0:T(8,128)(2,1)} %param.16, bf16[384,2048]{1,0:T(8,128)(2,1)} %all-gather.3.cloned.1.call-done, f32[2048]{0:T(1024)S(1)} %copy-done.8, ...), kind=kOutput, calls=%fused_computation.16 | convolution fusion | flops 1615724544 | bytes 8146432 | tf_op jit(solution)/shard_map/dot_general | solution.py:106
  101.2 19.4 %reduce-scatter.5.cloned.1.call-done = bf16[512,640]{0,1:T(8,128)(2,1)} async-done(((bf16[2048,640]{0,1:T(8,128)(2,1)}), bf16[512,640]{0,1:T(8,128)(2,1)}) %reduce-scatter.5.cloned.1.call-update) | async-done | bytes 655376 | tf_op jit(solution)/shard_map/reduce_scatter | solution.py:115
  120.6 5.5 %all-to-all-start.1 = ((bf16[512,1,8,80]{0,3,1,2:T(8,128)(2,1)}), bf16[512,1,8,80]{0,3,1,2:T(8,128)(2,1)}, u32[]{:S(2)}, u32[]{:S(2)}) async-start(bf16[512,1,8,80]{0,3,1,2:T(8,128)(2,1)} %bitcast.50), calls=%async_computation.3 | async-start | bytes 1310720 | tf_op jit(solution)/shard_map/all_to_all | solution.py:125
  126.3 1.0 eq.43
  127.3 16.0 %all-to-all-done.1 = bf16[512,1,8,80]{0,3,1,2:T(8,128)(2,1)} async-done(((bf16[512,1,8,80]{0,3,1,2:T(8,128)(2,1)}), bf16[512,1,8,80]{0,3,1,2:T(8,128)(2,1)}, u32[]{:S(2)}, u32[]{:S(2)}) %all-to-all-start.1) | async-done | bytes 655392 | tf_op jit(solution)/shard_map/all_to_all | solution.py:125
  143.3 2.3 %fusion.20 = bf16[512,160]{0,1:T(8,128)(2,1)} fusion(bf16[512,640,1]{0,1,2:T(8,128)(2,1)} %bitcast.18, pred[160,2,640]{2,1,0:T(4,128)(4,1)} %eq.43, f32[160,2]{0,1:T(2,128)S(1)} %divide_multiply_fusion), kind=kOutput, calls=%fused_computation.24 | convolution fusion | flops 209960960 | bytes 1025280 | tf_op jit(solution)/shard_map/dot_general | solution.py:127
  145.7 5.9 %reduce-scatter.3.cloned.1.call-done = bf16[512,384]{0,1:T(8,128)(2,1)} async-done(((bf16[2048,384]{0,1:T(8,128)(2,1)}), bf16[512,384]{0,1:T(8,128)(2,1)}) %reduce-scatter.3.cloned.1.call-update) | async-done | bytes 393232 | tf_op jit(solution)/shard_map/reduce_scatter | solution.py:105
  (40 shorter events, 1.0 us)
Async XLA Ops:
  7.2 63.2 %copy-start = (bf16[1,768,2048]{2,1,0:T(8,128)(2,1)S(1)}, bf16[1,768,2048]{2,1,0:T(8,128)(2,1)}, u32[]{:S(2)}) copy-start(bf16[1,768,2048]{2,1,0:T(8,128)(2,1)} %param.27) | copy-start | bytes 9437188
  7.2 55.2 %all-gather.5.cloned.1.call-start = ((), (), s32[]{:S(2)}) async-start(), calls=%async_computation.6 | async-start | bytes 3276800 | tf_op jit(solution)/shard_map/all_gather | solution.py:80
  38.0 26.9 %copy-start.7 = (f32[2048]{0:T(1024)S(1)}, f32[2048]{0:T(1024)}, u32[]{:S(2)}) copy-start(f32[2048]{0:T(1024)} %param.22) | copy-start | bytes 24580
  38.0 45.6 %all-gather.3.cloned.1.call-start = ((), (), s32[]{:S(2)}) async-start(), calls=%async_computation.4 | async-start | bytes 1966080 | tf_op jit(solution)/shard_map/all_gather | solution.py:77
  38.8 81.8 %reduce-scatter.5.cloned.1.call-start = ((), (), s32[]{:S(2)}) async-start(), calls=%async_computation.7 | async-start | bytes 3276800 | tf_op jit(solution)/shard_map/reduce_scatter | solution.py:115
  62.4 2.5 %copy-start.1 = (bf16[640,2048]{1,0:T(8,128)(2,1)S(1)}, bf16[640,2048]{1,0:T(8,128)(2,1)}, u32[]{:S(2)}) copy-start(bf16[640,2048]{1,0:T(8,128)(2,1)} %all-gather.5.cloned.1.call-done) | copy-start | bytes 7864324
  80.4 5.1 %copy-start.8 = (f32[2048]{0:T(1024)S(1)}, f32[2048]{0:T(1024)}, u32[]{:S(2)}) copy-start(f32[2048]{0:T(1024)} %param.15) | copy-start | bytes 24580
  80.4 71.2 %reduce-scatter.3.cloned.1.call-start = ((), (), s32[]{:S(2)}) async-start(), calls=%async_computation.5 | async-start | bytes 1966080 | tf_op jit(solution)/shard_map/reduce_scatter | solution.py:105
  85.4 3.2 %copy-start.2 = (bf16[384,2048]{1,0:T(8,128)(2,1)S(1)}, bf16[384,2048]{1,0:T(8,128)(2,1)}, u32[]{:S(2)}) copy-start(bf16[384,2048]{1,0:T(8,128)(2,1)} %all-gather.3.cloned.1.call-done) | copy-start | bytes 4718596
  85.4 3.2 %copy-start.6 = (bf16[2048,512]{1,0:T(8,128)(2,1)S(1)}, bf16[2048,512]{1,0:T(8,128)(2,1)}, u32[]{:S(2)}) copy-start(bf16[2048,512]{1,0:T(8,128)(2,1)} %param.17) | copy-start | bytes 6291460
  88.7 4.4 %copy-start.4 = (f32[3,512]{1,0:T(4,128)S(1)}, f32[3,512]{1,0:T(4,128)}, u32[]{:S(2)}) copy-start(f32[3,512]{1,0:T(4,128)} %param.19) | copy-start | bytes 18436
  89.7 4.7 %copy-start.5 = (f32[384,512]{1,0:T(8,128)}, f32[384,512]{1,0:T(8,128)S(1)}, u32[]{:S(2)}) copy-start(f32[384,512]{1,0:T(8,128)S(1)} %fusion.19) | copy-start | bytes 2359300
  89.7 4.7 %collective-permute-start = (f32[2,512]{1,0:T(2,128)S(1)}, f32[2,512]{1,0:T(2,128)S(1)}, u32[]{:S(2)}, u32[]{:S(2)}) collective-permute-start(f32[2,512]{1,0:T(2,128)S(1)} %slice.36), channel_id=1, source_target_pairs={{0,4},{4,8},{8,12},{12,16},{16,20},{20,24},{24,28},{1,5},{5,9},{9,... | collective-permute-start | bytes 12296 | tf_op jit(solution)/shard_map/ppermute | solution.py:13
  101.2 26.1 %copy-start.3 = (f32[160,2]{0,1:T(2,128)S(1)}, f32[160,2]{0,1:T(2,128)}, u32[]{:S(2)}) copy-start(f32[160,2]{0,1:T(2,128)} %param.24) | copy-start | bytes 3844
  120.6 22.7 %all-to-all-start.1 = ((bf16[512,1,8,80]{0,3,1,2:T(8,128)(2,1)}), bf16[512,1,8,80]{0,3,1,2:T(8,128)(2,1)}, u32[]{:S(2)}, u32[]{:S(2)}) async-start(bf16[512,1,8,80]{0,3,1,2:T(8,128)(2,1)} %bitcast.50), calls=%async_computation.3 | async-start | bytes 1310720 | tf_op jit(solution)/shard_map/all_to_all | solution.py:125
Sparse Core Ops, SparseCore 0:
  38.1 24.2 all-gather.4
  64.0 19.6 all-gather.2
  86.2 34.3 reduce-scatter.4
  123.5 27.9 reduce-scatter.2
where the time goes:
time: 158 us
  waiting for transfers between devices  70.1 us (44%)
  matrix products  30.3 us (19%)
  blocking collectives  24.9 us (16%)
  between operations  13.9 us (9%)
  starting transfers between devices  9.05 us (6%)
  other arithmetic  5.51 us (3%)
  local copies, waits for them, and re-layouts  4.3 us (3%)
    all_to_all x1, blocking collectives, local(): lax.all_to_all(outgoing, 'ep', split_axis=0, concat_axis=2, tiled=True)  24.9 us
    all_gather x1, waiting for transfers between devices, local(): lax.all_gather(arrived, 'tp', axis=1, tiled=True)  23.6 us
    reduce_scatter x1, waiting for transfers between devices, local(): lax.psum_scatter(summed.reshape(lax.axis_size('tp') * feature_local, loca...  19.4 us
    all_to_all x1, waiting for transfers between devices, local(): lax.all_to_all(returning, 'ep', split_axis=2, concat_axis=2, tiled=True)  16 us
    dot_general x1, matrix products, local(): jnp.einsum('gsf,gfd->dgs', activated, sliced, preferred_element_type=jnp....  9.98 us
    dot_general x3, matrix products, project_piece(): jnp.einsum('gsd,gdf->gsf', grouped, matrix, preferred_element_type=jnp.fl...  9.62 us
    dot_general x1, matrix products, local(): lax.dot_general(sliced, gated, (((0,), (1,)), ((), ())), preferred_elemen...  6.74 us
    reduce_scatter x1, waiting for transfers between devices, local(): lax.psum_scatter(lax.dot_general(sliced, gated, (((0,), (1,)), ((), ())),...  5.88 us
  transfers between devices with their start and end apart: 6, of which 6 were waited for; matrix products, arithmetic and copies ran while one was open for 22% of the time, Pallas kernels for 0%

commit v1 on v0

--- a/solution.py
+++ b/solution.py
@@ -5,6 +5,29 @@
 
 epsilon = 1e-06
 routed_scale = 2.5
+
+
+def in_blocks(x, dim, peers):
+    before, after = (x.shape[:dim], x.shape[dim + 1 :])
+    return jnp.moveaxis(x.reshape(*before, peers, -1, *after), dim, 0)
+
+
+def joined_along(pieces, dim):
+    pieces = jnp.moveaxis(pieces, 0, dim)
+    dims = pieces.shape
+    return pieces.reshape(*dims[:dim], dims[dim] * dims[dim + 1], *dims[dim + 2 :])
+
+
+def rotated_exchange(shard, axis, split_dim, concat_dim):
+    peers, position = (lax.axis_size(axis), lax.axis_index(axis))
+    blocks = in_blocks(shard, split_dim, peers)
+    out = blocks
+    for turn in range(1, peers):
+        target, source = ((position + turn) % peers, (position - turn) % peers)
+        sent = lax.dynamic_index_in_dim(blocks, target, 0)
+        received = lax.ppermute(sent, axis, [(i, (i + turn) % peers) for i in range(peers)])
+        out = lax.dynamic_update_slice_in_dim(out, received, source, axis=0)
+    return joined_along(out, concat_dim)
 
 
 def passed_along(block, axis, distance):
@@ -69,7 +92,7 @@
         send_table, repeated, (((0,), (0,)), ((), ())), preferred_element_type=jnp.float32
     ).astype(jnp.bfloat16)
     outgoing = outgoing.reshape(ep_count, local_experts, capacity, feature_local)
-    arrived = lax.all_to_all(outgoing, "ep", split_axis=0, concat_axis=2, tiled=True)
+    arrived = rotated_exchange(outgoing, "ep", 0, 2)
     arrived = arrived.reshape(local_experts * slot_rows, feature_local)
     mix_weights = (gate_b_weight[None], gate_c_weight[None], value_weight[None])
     expert_weights = (expert_gate, expert_up)

time: 158 us -> 164 us (1.038)
  blocking collectives: 24.9 us -> 0 us
  starting transfers between devices: 9.05 us -> 20.4 us
  waiting for transfers between devices: 70.1 us -> 81.3 us
  local copies, waits for them, and re-layouts: 4.3 us -> 11.8 us
    all_to_all x1 -> x0, blocking collectives: 24.9 us -> none  [local(): lax.all_to_all(outgoing, 'ep', split_axis=0, concat_axis=2, tiled=True)]
    ppermute x0 -> x7, starting transfers between devices: none -> 11.2 us  [rotated_exchange(): lax.ppermute(sent, axis, [(i, (i + turn) % peers) for i in range(peers)])]
    ppermute x0 -> x7, waiting for transfers between devices: none -> 8.04 us  [rotated_exchange(): lax.ppermute(sent, axis, [(i, (i + turn) % peers) for i in range(peers)])]
    dynamic_update_slice x0 -> x6, local copies, waits for them, and re-layouts: none -> 4.73 us  [rotated_exchange(): out = lax.dynamic_update_slice_in_dim(out, received, source, axis=0)]
    all_gather x1, waiting for transfers between devices: 23.6 us -> 26.9 us  [local(): lax.all_gather(arrived, 'tp', axis=1, tiled=True)]
    dynamic_slice x0 -> x2, local copies, waits for them, and re-layouts: none -> 1.83 us  [rotated_exchange(): sent = lax.dynamic_index_in_dim(blocks, target, 0)]
  transfers between devices with their start and end apart: 6 -> 13, of which waited for: 6 -> 8; matrix products, arithmetic and copies ran while one was open for 22% -> 23% of each run, Pallas kernels for 0% -> 0%
where the time goes in v1:
time: 164 us; the launch traced here: 163 us
  waiting for transfers between devices  81.3 us (50%)
  matrix products  30.3 us (18%)
  starting transfers between devices  20.4 us (12%)
  between operations  14 us (9%)
  local copies, waits for them, and re-layouts  11.8 us (7%)
  other arithmetic  5.51 us (3%)
    all_gather x1, waiting for transfers between devices, local(): lax.all_gather(arrived, 'tp', axis=1, tiled=True)  26.9 us
    reduce_scatter x1, waiting for transfers between devices, local(): lax.psum_scatter(summed.reshape(lax.axis_size('tp') * feature_local, loca...  19.4 us
    all_to_all x1, waiting for transfers between devices, local(): lax.all_to_all(returning, 'ep', split_axis=2, concat_axis=2, tiled=True)  16 us
    ppermute x7, starting transfers between devices, rotated_exchange(): lax.ppermute(sent, axis, [(i, (i + turn) % peers) for i in range(peers)])  11.2 us
    dot_general x1, matrix products, local(): jnp.einsum('gsf,gfd->dgs', activated, sliced, preferred_element_type=jnp....  9.97 us
    dot_general x3, matrix products, project_piece(): jnp.einsum('gsd,gdf->gsf', grouped, matrix, preferred_element_type=jnp.fl...  9.64 us
    ppermute x7, waiting for transfers between devices, rotated_exchange(): lax.ppermute(sent, axis, [(i, (i + turn) % peers) for i in range(peers)])  8.04 us
    dot_general x1, matrix products, local(): lax.dot_general(sliced, gated, (((0,), (1,)), ((), ())), preferred_elemen...  6.75 us
  transfers between devices with their start and end apart: 13, of which 8 were waited for; matrix products, arithmetic and copies ran while one was open for 23% of the time, Pallas kernels for 0%

profile of v1, /device:TPU:0, one launch (start us, length us, event | category | flops | bytes accessed | tf_op | source)
XLA Modules:
  0.0 163.2 jit_solution(13776471515225128158)
XLA Ops:
  11.5 1.6 convolution_convert_fusion.2
  14.0 3.0 %collective-permute-start.1 = (bf16[1,1,1,80,512]{4,3,0,2,1:T(8,128)(2,1)S(1)}, bf16[1,1,1,80,512]{4,3,0,2,1:T(8,128)(2,1)}, u32[]{:S(2)}, u32[]{:S(2)}) collective-permute-start(bf16[1,1,1,80,512]{4,3,0,2,1:T(8,128)(2,1)S(1)} %constant_dynamic-slice_fusion.6), channel_id=1, source_target_pairs={{0,4},{4,8},{8,12},{12,16},{16,20},{20,24},{24,28},{28,0},{1,5},{5... | collective-permute-start | bytes 245768 | tf_op jit(solution)/shard_map/ppermute | solution.py:28
  17.0 5.6 %collective-permute-done.1 = bf16[1,1,1,80,512]{4,3,0,2,1:T(8,128)(2,1)} collective-permute-done((bf16[1,1,1,80,512]{4,3,0,2,1:T(8,128)(2,1)S(1)}, bf16[1,1,1,80,512]{4,3,0,2,1:T(8,128)(2,1)}, u32[]{:S(2)}, u32[]{:S(2)}) %collective-permute-start.1) | collective-permute-done | bytes 81952 | tf_op jit(solution)/shard_map/ppermute | solution.py:28
  22.6 1.8 %constant_dynamic-slice_fusion = (bf16[1,1,1,80,512]{4,3,0,2,1:T(8,128)(2,1)S(1)}, bf16[1,1,1,80,512]{4,3,0,2,1:T(8,128)(2,1)S(1)}, bf16[1,1,1,80,512]{4,3,0,2,1...) fusion(bf16[8,1,1,80,512]{4,3,0,2,1:T(8,128)(2,1)} %bitcast.48,, ...), kind=kLoop, calls=%fused_computation.54 | loop fusion | bytes 1146908 | tf_op jit(solution)/shard_map/jit(dynamic_index_in_dim)/dynamic_slice | solution.py:27
  24.4 1.5 collective-permute-start.3
  26.0 1.2 collective-permute-start.4
  27.2 3.6 %collective-permute-start.5 = (bf16[1,1,1,80,512]{4,3,0,2,1:T(8,128)(2,1)S(1)}, bf16[1,1,1,80,512]{4,3,0,2,1:T(8,128)(2,1)S(1)}, u32[]{:S(2)}, u32[]{:S(2)}) collective-permute-start(bf16[1,1,1,80,512]{4,3,0,2,1:T(8,128)(2,1)S(1)} %get-tuple-element.4), channel_id=1, source_target_pairs={{0,20},{4,24},{8,28},{12,0},{16,4},{20,8},{24,12},{28,16},{1,21},{... | collective-permute-start | bytes 245768 | tf_op jit(solution)/shard_map/ppermute | solution.py:28
  30.8 1.3 collective-permute-start.6
  32.6 1.5 constant_dynamic-update-slice_fusion.5
  34.8 2.4 %collective-permute-done.4 = bf16[1,1,1,80,512]{4,3,0,2,1:T(8,128)(2,1)S(1)} collective-permute-done((bf16[1,1,1,80,512]{4,3,0,2,1:T(8,128)(2,1)S(1)}, bf16[1,1,1,80,512]{4,3,0,2,1:T(8,128)(2,1)S(1)}, u32[]{:S(2)}, u32[]{:S(2)}) %collective-permute-start.4) | collective-permute-done | bytes 81952 | tf_op jit(solution)/shard_map/ppermute | solution.py:28
  40.6 26.9 %all-gather.5.cloned.1.call-done = bf16[640,2048]{1,0:T(8,128)(2,1)} async-done(((bf16[640,512]{1,0:T(8,128)(2,1)}), bf16[640,2048]{1,0:T(8,128)(2,1)}) %all-gather.5.cloned.1.call-update) | async-done | bytes 2621456 | tf_op jit(solution)/shard_map/all_gather | solution.py:103
  67.5 2.5 %fusion.1 = f32[640]{0:T(1024)S(1)} fusion(bf16[640,2048]{1,0:T(8,128)(2,1)} %all-gather.5.cloned.1.call-done), kind=kLoop, calls=%fused_computation.3 | loop fusion | flops 3931520 | bytes 2624000 | tf_op jit(solution)/shard_map/reduce_sum | solution.py:50
  70.1 5.4 %fusion.7 = f32[640,768]{1,0:T(8,128)} fusion(bf16[1,2048,768]{2,1,0:T(8,128)(2,1)} %param.25, bf16[640,2048]{1,0:T(8,128)(2,1)S(1)} %copy-done.1, f32[2048]{0:T(1024)S(1)} %copy-done.10), kind=kOutput, calls=%fused_computation.12 | convolution fusion | flops 2017198080 | bytes 7741440 | tf_op jit(solution)/shard_map/gsd,gdf->gsf/dot_general | solution.py:46
  75.5 10.0 %fusion.9 = bf16[2048,640]{0,1:T(8,128)(2,1)} fusion(bf16[1,768,2048]{2,1,0:T(8,128)(2,1)S(1)} %copy-done, f32[640,768]{1,0:T(8,128)} %fusion.7, bf16[1,2048,768]{2,1,0:T(8,128)(2,1)} %param.26, bf16[640,2048]{1,0:T(8,128)(2,1)} %all-gather.5.cloned.1.call-done, f32[2048]{0:T(1024)S(1)} %copy-done.10, f32[640]{0:T(1024)S(1)} %add_rsqrt_fusion), kind=kOutput, calls=%fused_computation.14 | convolution fusion | flops 4035706880 | bytes 13511168 | tf_op jit(solution)/shard_map/gsf,gfd->dgs/dot_general | solution.py:137
  85.6 3.2 %all-gather.3.cloned.1.call-done = bf16[384,2048]{1,0:T(8,128)(2,1)} async-done(((bf16[384,512]{1,0:T(8,128)(2,1)}), bf16[384,2048]{1,0:T(8,128)(2,1)}) %all-gather.3.cloned.1.call-update) | async-done | bytes 1572880 | tf_op jit(solution)/shard_map/all_gather | solution.py:100
  88.8 1.8 %fusion.3 = f32[384]{0:T(512)S(1)} fusion(bf16[384,2048]{1,0:T(8,128)(2,1)} %all-gather.3.cloned.1.call-done), kind=kLoop, calls=%fused_computation.8 | loop fusion | flops 2358912 | bytes 1574400 | tf_op jit(solution)/shard_map/reduce_sum | solution.py:50
  90.6 3.2 %convolution_multiply_fusion = f32[384,512]{1,0:T(8,128)S(1)} fusion(bf16[2048,512]{1,0:T(8,128)(2,1)} %param.18, bf16[384,2048]{1,0:T(8,128)(2,1)} %all-gather.3.cloned.1.call-done, f32[2048]{0:T(1024)S(1)} %copy-done.11, f32[384]{0:T(512)S(1)} %add_rsqrt_fusion.1), kind=kOutput, calls=%fused_computation.19 | convolution fusion | flops 807862272 | bytes 4466176 | tf_op jit(solution)/shard_map/gsd,gdf->gsf/dot_general | solution.py:46
  94.9 3.5 %collective-permute-start = (f32[2,512]{1,0:T(2,128)S(1)}, f32[2,512]{1,0:T(2,128)S(1)}, u32[]{:S(2)}, u32[]{:S(2)}) collective-permute-start(f32[2,512]{1,0:T(2,128)S(1)} %slice.36), channel_id=1, source_target_pairs={{0,4},{4,8},{8,12},{12,16},{16,20},{20,24},{24,28},{1,5},{5,9},{9,... | collective-permute-start | bytes 12296 | tf_op jit(solution)/shard_map/ppermute | solution.py:36
  99.6 6.7 %fusion.12 = bf16[2048,384]{0,1:T(8,128)(2,1)} fusion(bf16[512,2048]{1,0:T(8,128)(2,1)} %param.20, f32[2,512]{1,0:T(2,128)S(1)} %collective-permute-done, f32[384,512]{1,0:T(8,128)} %copy-done.8, bf16[2048,512]{1,0:T(8,128)(2,1)} %param.16, bf16[384,2048]{1,0:T(8,128)(2,1)} %all-gather.3.cloned.1.call-done, f32[2048]{0:T(1024)S(1)} %copy-done.11, ...), kind=kOutput, calls=%fused_computation.16 | convolution fusion | flops 1615724544 | bytes 8146432 | tf_op jit(solution)/shard_map/dot_general | solution.py:129
  106.3 19.4 %reduce-scatter.5.cloned.1.call-done = bf16[512,640]{0,1:T(8,128)(2,1)} async-done(((bf16[2048,640]{0,1:T(8,128)(2,1)}), bf16[512,640]{0,1:T(8,128)(2,1)}) %reduce-scatter.5.cloned.1.call-update) | async-done | bytes 655376 | tf_op jit(solution)/shard_map/reduce_scatter | solution.py:138
  125.7 5.5 %all-to-all-start = ((bf16[512,1,8,80]{0,3,1,2:T(8,128)(2,1)}), bf16[512,1,8,80]{0,3,1,2:T(8,128)(2,1)}, u32[]{:S(2)}, u32[]{:S(2)}) async-start(bf16[512,1,8,80]{0,3,1,2:T(8,128)(2,1)} %bitcast.50), calls=%async_computation.2 | async-start | bytes 1310720 | tf_op jit(solution)/shard_map/all_to_all | solution.py:148
  132.5 16.0 %all-to-all-done = bf16[512,1,8,80]{0,3,1,2:T(8,128)(2,1)} async-done(((bf16[512,1,8,80]{0,3,1,2:T(8,128)(2,1)}), bf16[512,1,8,80]{0,3,1,2:T(8,128)(2,1)}, u32[]{:S(2)}, u32[]{:S(2)}) %all-to-all-start) | async-done | bytes 655392 | tf_op jit(solution)/shard_map/all_to_all | solution.py:148
  148.5 2.3 %fusion.20 = bf16[512,160]{0,1:T(8,128)(2,1)} fusion(bf16[512,640,1]{0,1,2:T(8,128)(2,1)} %bitcast.17, pred[160,2,640]{2,1,0:T(4,128)(4,1)} %eq.58, f32[160,2]{0,1:T(2,128)S(1)} %divide_multiply_fusion), kind=kOutput, calls=%fused_computation.24 | convolution fusion | flops 209960960 | bytes 1025280 | tf_op jit(solution)/shard_map/dot_general | solution.py:150
  150.8 5.9 %reduce-scatter.3.cloned.1.call-done = bf16[512,384]{0,1:T(8,128)(2,1)} async-done(((bf16[2048,384]{0,1:T(8,128)(2,1)}), bf16[512,384]{0,1:T(8,128)(2,1)}) %reduce-scatter.3.cloned.1.call-update) | async-done | bytes 393232 | tf_op jit(solution)/shard_map/reduce_scatter | solution.py:128
  (67 shorter events, 13.2 us)
Async XLA Ops:
  7.2 68.4 %copy-start = (bf16[1,768,2048]{2,1,0:T(8,128)(2,1)S(1)}, bf16[1,768,2048]{2,1,0:T(8,128)(2,1)}, u32[]{:S(2)}) copy-start(bf16[1,768,2048]{2,1,0:T(8,128)(2,1)} %param.27) | copy-start | bytes 9437188
  7.2 60.4 %all-gather.5.cloned.1.call-start = ((), (), s32[]{:S(2)}) async-start(), calls=%async_computation.5 | async-start | bytes 3276800 | tf_op jit(solution)/shard_map/all_gather | solution.py:103
  9.6 7.4 %copy-start.4 = (s32[320]{0:T(512)}, s32[320]{0:T(512)S(1)}, u32[]{:S(2)}) copy-start(s32[320]{0:T(512)S(1)} %multiply_add_fusion) | copy-start | bytes 3844
  14.0 8.6 %collective-permute-start.1 = (bf16[1,1,1,80,512]{4,3,0,2,1:T(8,128)(2,1)S(1)}, bf16[1,1,1,80,512]{4,3,0,2,1:T(8,128)(2,1)}, u32[]{:S(2)}, u32[]{:S(2)}) collective-permute-start(bf16[1,1,1,80,512]{4,3,0,2,1:T(8,128)(2,1)S(1)} %constant_dynamic-slice_fusion.6), channel_id=1, source_target_pairs={{0,4},{4,8},{8,12},{12,16},{16,20},{20,24},{24,28},{28,0},{1,5},{5... | collective-permute-start | bytes 245768 | tf_op jit(solution)/shard_map/ppermute | solution.py:28
  24.4 7.7 %collective-permute-start.2 = (bf16[1,1,1,80,512]{4,3,0,2,1:T(8,128)(2,1)}, bf16[1,1,1,80,512]{4,3,0,2,1:T(8,128)(2,1)}, u32[]{:S(2)}, u32[]{:S(2)}) collective-permute-start(bf16[1,1,1,80,512]{4,3,0,2,1:T(8,128)(2,1)} %get-tuple-element.7), channel_id=1, source_target_pairs={{0,8},{4,12},{8,16},{12,20},{16,24},{20,28},{24,0},{28,4},{1,9},{5... | collective-permute-start | bytes 245768 | tf_op jit(solution)/shard_map/ppermute | solution.py:28
  24.4 9.7 %collective-permute-start.3 = (bf16[1,1,1,80,512]{4,3,0,2,1:T(8,128)(2,1)S(1)}, bf16[1,1,1,80,512]{4,3,0,2,1:T(8,128)(2,1)S(1)}, u32[]{:S(2)}, u32[]{:S(2)}) collective-permute-start(bf16[1,1,1,80,512]{4,3,0,2,1:T(8,128)(2,1)S(1)} %get-tuple-element.6), channel_id=1, source_target_pairs={{0,12},{4,16},{8,20},{12,24},{16,28},{20,0},{24,4},{28,8},{1,13},{... | collective-permute-start | bytes 245768 | tf_op jit(solution)/shard_map/ppermute | solution.py:28
  26.0 11.3 %collective-permute-start.4 = (bf16[1,1,1,80,512]{4,3,0,2,1:T(8,128)(2,1)S(1)}, bf16[1,1,1,80,512]{4,3,0,2,1:T(8,128)(2,1)S(1)}, u32[]{:S(2)}, u32[]{:S(2)}) collective-permute-start(bf16[1,1,1,80,512]{4,3,0,2,1:T(8,128)(2,1)S(1)} %get-tuple-element.5), channel_id=1, source_target_pairs={{0,16},{4,20},{8,24},{12,28},{16,0},{20,4},{24,8},{28,12},{1,17},{... | collective-permute-start | bytes 245768 | tf_op jit(solution)/shard_map/ppermute | solution.py:28
  27.2 10.7 %collective-permute-start.5 = (bf16[1,1,1,80,512]{4,3,0,2,1:T(8,128)(2,1)S(1)}, bf16[1,1,1,80,512]{4,3,0,2,1:T(8,128)(2,1)S(1)}, u32[]{:S(2)}, u32[]{:S(2)}) collective-permute-start(bf16[1,1,1,80,512]{4,3,0,2,1:T(8,128)(2,1)S(1)} %get-tuple-element.4), channel_id=1, source_target_pairs={{0,20},{4,24},{8,28},{12,0},{16,4},{20,8},{24,12},{28,16},{1,21},{... | collective-permute-start | bytes 245768 | tf_op jit(solution)/shard_map/ppermute | solution.py:28
  30.8 7.8 %collective-permute-start.6 = (bf16[1,1,1,80,512]{4,3,0,2,1:T(8,128)(2,1)S(1)}, bf16[1,1,1,80,512]{4,3,0,2,1:T(8,128)(2,1)S(1)}, u32[]{:S(2)}, u32[]{:S(2)}) collective-permute-start(bf16[1,1,1,80,512]{4,3,0,2,1:T(8,128)(2,1)S(1)} %get-tuple-element.3), channel_id=1, source_target_pairs={{0,24},{4,28},{8,0},{12,4},{16,8},{20,12},{24,16},{28,20},{1,25},{... | collective-permute-start | bytes 245768 | tf_op jit(solution)/shard_map/ppermute | solution.py:28
  32.1 7.1 %collective-permute-start.7 = (bf16[1,1,1,80,512]{4,3,0,2,1:T(8,128)(2,1)S(1)}, bf16[1,1,1,80,512]{4,3,0,2,1:T(8,128)(2,1)S(1)}, u32[]{:S(2)}, u32[]{:S(2)}) collective-permute-start(bf16[1,1,1,80,512]{4,3,0,2,1:T(8,128)(2,1)S(1)} %get-tuple-element.2), channel_id=1, source_target_pairs={{0,28},{4,0},{8,4},{12,8},{16,12},{20,16},{24,20},{28,24},{1,29},{... | collective-permute-start | bytes 245768 | tf_op jit(solution)/shard_map/ppermute | solution.py:28
  37.9 32.1 %copy-start.10 = (f32[2048]{0:T(1024)S(1)}, f32[2048]{0:T(1024)}, u32[]{:S(2)}) copy-start(f32[2048]{0:T(1024)} %param.22) | copy-start | bytes 24580
  39.8 48.9 %all-gather.3.cloned.1.call-start = ((), (), s32[]{:S(2)}) async-start(), calls=%async_computation.3 | async-start | bytes 1966080 | tf_op jit(solution)/shard_map/all_gather | solution.py:100
  40.6 85.1 %reduce-scatter.5.cloned.1.call-start = ((), (), s32[]{:S(2)}) async-start(), calls=%async_computation.6 | async-start | bytes 3276800 | tf_op jit(solution)/shard_map/reduce_scatter | solution.py:138
  67.5 2.5 %copy-start.1 = (bf16[640,2048]{1,0:T(8,128)(2,1)S(1)}, bf16[640,2048]{1,0:T(8,128)(2,1)}, u32[]{:S(2)}) copy-start(bf16[640,2048]{1,0:T(8,128)(2,1)} %all-gather.5.cloned.1.call-done) | copy-start | bytes 7864324
  85.5 5.1 %copy-start.11 = (f32[2048]{0:T(1024)S(1)}, f32[2048]{0:T(1024)}, u32[]{:S(2)}) copy-start(f32[2048]{0:T(1024)} %param.15) | copy-start | bytes 24580
  85.5 71.2 %reduce-scatter.3.cloned.1.call-start = ((), (), s32[]{:S(2)}) async-start(), calls=%async_computation.4 | async-start | bytes 1966080 | tf_op jit(solution)/shard_map/reduce_scatter | solution.py:128
  90.6 3.2 %copy-start.3 = (bf16[384,2048]{1,0:T(8,128)(2,1)S(1)}, bf16[384,2048]{1,0:T(8,128)(2,1)}, u32[]{:S(2)}) copy-start(bf16[384,2048]{1,0:T(8,128)(2,1)} %all-gather.3.cloned.1.call-done) | copy-start | bytes 4718596
  90.6 3.2 %copy-start.9 = (bf16[2048,512]{1,0:T(8,128)(2,1)S(1)}, bf16[2048,512]{1,0:T(8,128)(2,1)}, u32[]{:S(2)}) copy-start(bf16[2048,512]{1,0:T(8,128)(2,1)} %param.17) | copy-start | bytes 6291460
  93.8 4.6 %copy-start.7 = (f32[3,512]{1,0:T(4,128)S(1)}, f32[3,512]{1,0:T(4,128)}, u32[]{:S(2)}) copy-start(f32[3,512]{1,0:T(4,128)} %param.19) | copy-start | bytes 18436
  94.8 4.7 %copy-start.8 = (f32[384,512]{1,0:T(8,128)}, f32[384,512]{1,0:T(8,128)S(1)}, u32[]{:S(2)}) copy-start(f32[384,512]{1,0:T(8,128)S(1)} %fusion.19) | copy-start | bytes 2359300
  94.9 4.7 %collective-permute-start = (f32[2,512]{1,0:T(2,128)S(1)}, f32[2,512]{1,0:T(2,128)S(1)}, u32[]{:S(2)}, u32[]{:S(2)}) collective-permute-start(f32[2,512]{1,0:T(2,128)S(1)} %slice.36), channel_id=1, source_target_pairs={{0,4},{4,8},{8,12},{12,16},{16,20},{20,24},{24,28},{1,5},{5,9},{9,... | collective-permute-start | bytes 12296 | tf_op jit(solution)/shard_map/ppermute | solution.py:36
  106.3 24.9 %copy-start.5 = (s32[320]{0:T(512)S(1)}, s32[320]{0:T(512)}, u32[]{:S(2)}) copy-start(s32[320]{0:T(512)} %copy-done.4) | copy-start | bytes 3844
  106.3 26.1 %copy-start.6 = (f32[160,2]{0,1:T(2,128)S(1)}, f32[160,2]{0,1:T(2,128)}, u32[]{:S(2)}) copy-start(f32[160,2]{0,1:T(2,128)} %param.24) | copy-start | bytes 3844
  125.7 22.7 %all-to-all-start = ((bf16[512,1,8,80]{0,3,1,2:T(8,128)(2,1)}), bf16[512,1,8,80]{0,3,1,2:T(8,128)(2,1)}, u32[]{:S(2)}, u32[]{:S(2)}) async-start(bf16[512,1,8,80]{0,3,1,2:T(8,128)(2,1)} %bitcast.50), calls=%async_computation.2 | async-start | bytes 1310720 | tf_op jit(solution)/shard_map/all_to_all | solution.py:148
  (1 other events, 0.9 us)
Sparse Core Ops, SparseCore 0:
  40.0 27.5 all-gather.4
  69.1 19.6 all-gather.2
  91.3 34.3 reduce-scatter.4
  128.7 27.9 reduce-scatter.2
